TPU v7x, 32 devices: a whole 2x2x4 slice. The times are simulated.
32 devices in a mesh: fs: 16 (over z, y, x), tp: 2 (over core).
Axes of the slice: x: 2, y: 2, z: 4, core: 2. Of those that a mesh axis runs over, the one named last changes fastest.
Arguments:
- inputs: bfloat16 [8192, 2048], P('fs', 'tp'), may hold values from -6 to 6
- value_cotangent: bfloat16 [8192, 2048], P('fs', 'tp'), may hold values from -6 to 6
- first_map: bfloat16 [8192, 2048], P('fs', 'tp'), may hold values from -6 to 6
- second_map: bfloat16 [8192, 2048], P('fs', 'tp'), may hold values from -6 to 6
- lambdas: float32 [16], P('tp'), may hold values from 0.3 to 0.8
- head_gain: float32 [128], replicated, may hold values from 0.1 to 1.9
- output_cotangent: bfloat16 [8192, 2048], P('fs', 'tp'), may hold values from -6 to 6
- value_factor: bfloat16 [2048, 256], replicated, may hold values from -0.125 to 0.125
- output_factor: bfloat16 [2048, 256], replicated, may hold values from -0.125 to 0.125
- value_weight: float32 [2048, 2048], P('fs', 'tp'), may hold values from -0.125 to 0.125
- output_weight: float32 [2048, 2048], P('tp', 'fs'), may hold values from -0.125 to 0.125
- value_moment: float32 [256, 2048], P('fs', 'tp'), may hold values from -6 to 6
- value_second: float32 [256, 2048], P('fs', 'tp'), may hold values from 0.25 to 4
- output_moment: float32 [256, 2048], P('fs', 'tp'), may hold values from -6 to 6
- output_second: float32 [256, 2048], P('fs', 'tp'), may hold values from 0.25 to 4
Outputs:
- value_master: float32 [2048, 2048], P('fs', 'tp')
- output_master: float32 [2048, 2048], P('tp', 'fs')
- value_moment_new: float32 [256, 2048], P('fs', 'tp')
- value_second_new: float32 [256, 2048], P('fs', 'tp')
- output_moment_new: float32 [256, 2048], P('fs', 'tp')
- output_second_new: float32 [256, 2048], P('fs', 'tp')
- value_copy: bfloat16 [2048, 2048], P(None, 'tp')
- output_copy: bfloat16 [2048, 2048], P('tp')
All inputs are finite; a program needn't handle non-finite values.
Results may differ from a plain program's by a relative error of at most 0.0027.
Values may be sent and summed in bfloat16 or wider, within the bound.
A program may use at most 64 MiB of HBM per device.

v0:
```python
import math
import jax
import jax.numpy as jnp
from jax import lax
from jax.sharding import PartitionSpec as P


def contract_rows(left, right, precise):
    if precise:
        return lax.dot_general(
            left,
            right,
            (((0,), (0,)), ((), ())),
            precision=lax.Precision.HIGHEST,
            preferred_element_type=jnp.float32,
        )
    return lax.dot_general(
        left, right, (((0,), (0,)), ((), ())), preferred_element_type=jnp.float32
    )


def local(
    inputs,
    value_cotangent,
    first_map,
    second_map,
    lambdas,
    head_gain,
    output_cotangent,
    value_factor,
    output_factor,
    value_weight,
    output_weight,
    value_moment,
    value_second,
    output_moment,
    output_second,
):
    tok_rows = inputs.shape[0]
    local_heads = lambdas.shape[0]
    head_width = head_gain.shape[0]
    head_cols = local_heads * head_width
    first = first_map.astype(jnp.float32).reshape(tok_rows, local_heads, head_width)
    second = second_map.astype(jnp.float32).reshape(tok_rows, local_heads, head_width)
    difference = first - lambdas[None, :, None] * second
    normed = (
        difference
        * lax.rsqrt(jnp.mean(difference * difference, axis=-1, keepdims=True) + 1e-06)
        * head_gain
    )
    heads_out = normed.reshape(tok_rows, head_cols).astype(jnp.bfloat16)
    full_inputs, full_cotangent = (
        lax.all_gather(inputs, "tp", axis=1, tiled=True),
        lax.all_gather(output_cotangent, "tp", axis=1, tiled=True),
    )
    token_scale = 1.0 / math.sqrt(tok_rows * lax.axis_size("fs"))
    fs_index = lax.axis_index("fs")
    width_rows = value_weight.shape[0]
    value_rows = lax.dynamic_slice_in_dim(
        value_factor, fs_index * width_rows, width_rows, 0
    ).astype(jnp.float32)
    output_rows = lax.dynamic_slice_in_dim(
        output_factor, fs_index * width_rows, width_rows, 0
    ).astype(jnp.float32)
    grad_value = contract_rows(full_inputs, value_cotangent, False) * token_scale
    grad_output = contract_rows(full_cotangent, heads_out, False) * token_scale
    partial_value = jnp.concatenate(
        [
            contract_rows(value_factor.astype(jnp.float32), grad_value, True),
            contract_rows(output_factor.astype(jnp.float32), grad_output, True),
        ],
        axis=1,
    )
    own_rows = lax.psum_scatter(partial_value, "fs", scatter_dimension=0, tiled=True)
    moments = jnp.concatenate([value_moment, output_moment], axis=1)
    seconds = jnp.concatenate([value_second, output_second], axis=1)
    moment_new = 0.8 * moments + 0.2 * own_rows
    second_new = 0.95 * seconds + 0.05 * own_rows * own_rows
    direction = moment_new / (jnp.sqrt(second_new) + 1e-08)
    full_direction = lax.all_gather(direction, "fs", axis=0, tiled=True)
    step_value = jnp.dot(
        value_rows,
        full_direction[:, :head_cols],
        precision=lax.Precision.HIGHEST,
        preferred_element_type=jnp.float32,
    )
    step_output = jnp.dot(
        output_rows,
        full_direction[:, head_cols:],
        precision=lax.Precision.HIGHEST,
        preferred_element_type=jnp.float32,
    )
    value_master = value_weight - 0.05 * step_value
    output_master = output_weight - 0.05 * step_output.T
    value_copy, output_copy = (
        lax.all_gather(value_master.astype(jnp.bfloat16), "fs", axis=0, tiled=True),
        lax.all_gather(output_master.astype(jnp.bfloat16), "fs", axis=1, tiled=True),
    )
    return (
        value_master,
        output_master,
        moment_new[:, :head_cols],
        second_new[:, :head_cols],
        moment_new[:, head_cols:],
        second_new[:, head_cols:],
        value_copy,
        output_copy,
    )


def solution(mesh):
    in_specs = (
        P("fs", "tp"),
        P("fs", "tp"),
        P("fs", "tp"),
        P("fs", "tp"),
        P("tp"),
        P(),
        P("fs", "tp"),
        P(),
        P(),
        P("fs", "tp"),
        P("tp", "fs"),
        P("fs", "tp"),
        P("fs", "tp"),
        P("fs", "tp"),
        P("fs", "tp"),
    )
    out_specs = (
        P("fs", "tp"),
        P("tp", "fs"),
        P("fs", "tp"),
        P("fs", "tp"),
        P("fs", "tp"),
        P("fs", "tp"),
        P(None, "tp"),
        P("tp", None),
    )
    return jax.shard_map(local, mesh=mesh, in_specs=in_specs, out_specs=out_specs, check_vma=False)
```

profile of v0, /device:TPU:0, one launch (start us, length us, event | category | flops | bytes accessed | tf_op | source)
XLA Modules:
  0.0 374.0 jit_solution(844891537116236253)
XLA Ops:
  7.2 0.7 all-gather.8.cloned.1.call-update
  8.0 0.7 all-gather.6.cloned.1.call-update
  9.5 0.7 copy-done.2
  11.4 0.6 multiply_reduce_fusion
  12.4 10.5 %all-gather.8.cloned.1.call-done = bf16[512,2048]{1,0:T(8,128)(2,1)} async-done(((bf16[512,1024]{1,0:T(8,128)(2,1)}), bf16[512,2048]{1,0:T(8,128)(2,1)}) %all-gather.8.cloned.1.call-update) | async-done | bytes 2097168 | tf_op jit(solution)/shard_map/all_gather | solution.py:54
  22.9 0.6 mul.105
  23.5 1.0 copy-done.5
  24.5 2.8 fusion.18
  27.3 4.0 %fusion.13 = f32[256,1024]{0,1:T(8,128)S(1)} fusion(bf16[2048,256]{1,0:T(8,128)(2,1)S(1)} %copy-done.8, f32[1024,2048]{1,0:T(8,128)S(1)} %fusion.18), kind=kOutput, calls=%fused_computation.18 | convolution fusion | flops 6444548096 | bytes 10485760 | tf_op jit(solution)/shard_map/dot_general | solution.py:10
  31.4 4.8 %all-gather.6.cloned.1.call-done = bf16[512,2048]{1,0:T(8,128)(2,1)} async-done(((bf16[512,1024]{1,0:T(8,128)(2,1)}), bf16[512,2048]{1,0:T(8,128)(2,1)}) %all-gather.6.cloned.1.call-update) | async-done | bytes 2097168 | tf_op jit(solution)/shard_map/all_gather | solution.py:53
  36.2 4.0 %fusion.38 = f32[2048,1024]{1,0:T(8,128)S(1)} fusion(bf16[512,2048]{1,0:T(8,128)(2,1)} %all-gather.6.cloned.1.call-done, bf16[512,1024]{1,0:T(8,128)(2,1)S(1)} %copy-done), kind=kOutput, calls=%fused_computation.47 | convolution fusion | flops 2147483648 | bytes 11534336 | tf_op jit(solution)/shard_map/dot_general | solution.py:17
  40.2 6.9 %fusion.10 = f32[256,1024]{0,1:T(8,128)S(1)} fusion(bf16[2048,256]{1,0:T(8,128)(2,1)S(1)} %copy-done.7, f32[2048,1024]{1,0:T(8,128)S(1)} %fusion.38), kind=kOutput, calls=%fused_computation.17 | convolution fusion | flops 6444548096 | bytes 10485760 | tf_op jit(solution)/shard_map/dot_general | solution.py:10
  47.3 1.8 copy.49
  49.3 82.7 %reduce-scatter.4.cloned.1.call-done = f32[16,2048]{1,0:T(8,128)} async-done(((f32[256,2048]{1,0:T(8,128)}), f32[16,2048]{1,0:T(8,128)}) %reduce-scatter.4.cloned.1.call-update) | async-done | bytes 131088 | tf_op jit(solution)/shard_map/reduce_scatter | solution.py:74
  132.0 1.6 add_divide_fusion
  133.7 58.5 %all-gather.10.cloned.1.call-done = f32[256,2048]{1,0:T(8,128)} async-done(((f32[16,2048]{1,0:T(8,128)}), f32[256,2048]{1,0:T(8,128)}) %all-gather.10.cloned.1.call-update) | async-done | bytes 2097168 | tf_op jit(solution)/shard_map/all_gather | solution.py:80
  192.2 2.8 fusion.36
  195.1 2.7 fusion.37
  197.8 0.7 fusion.35
  198.5 0.7 fusion.34
  199.1 70.7 %all-gather.12.cloned.1.call-done = bf16[2048,1024]{1,0:T(8,128)(2,1)} async-done(((bf16[128,1024]{1,0:T(8,128)(2,1)}), bf16[2048,1024]{1,0:T(8,128)(2,1)}) %all-gather.12.cloned.1.call-update) | async-done | bytes 4194320 | tf_op jit(solution)/shard_map/all_gather | solution.py:96
  269.8 90.5 %all-gather.14.cloned.1.call-done = bf16[1024,2048]{1,0:T(8,128)(2,1)} async-done(((bf16[1024,128]{1,0:T(8,128)(2,1)}), bf16[1024,2048]{1,0:T(8,128)(2,1)}) %all-gather.14.cloned.1.call-update) | async-done | bytes 4194320 | tf_op jit(solution)/shard_map/all_gather | solution.py:97
  360.3 4.8 %copy.58 = bf16[2048,1024]{1,0:T(8,128)(2,1)} copy(bf16[2048,1024]{1,0:T(8,128)(2,1)} %all-gather.12.cloned.1.call-done) | data formatting | bytes 8388608
  365.1 2.0 copy.59
  (52 shorter events, 2.7 us)
Async XLA Ops:
  7.2 29.0 %copy-start = (bf16[512,1024]{1,0:T(8,128)(2,1)S(1)}, bf16[512,1024]{1,0:T(8,128)(2,1)}, u32[]{:S(2)}) copy-start(bf16[512,1024]{1,0:T(8,128)(2,1)} %param.16) | copy-start | bytes 3145732
  7.2 1.5 copy-start.3
  7.2 15.7 %all-gather.8.cloned.1.call-start = ((), (), s32[]{:S(2)}) async-start(), calls=%async_computation.2 | async-start | bytes 3145728 | tf_op jit(solution)/shard_map/all_gather | solution.py:54
  7.9 28.3 %all-gather.6.cloned.1.call-start = ((), (), s32[]{:S(2)}) async-start(), calls=%async_computation.1 | async-start | bytes 3145728 | tf_op jit(solution)/shard_map/all_gather | solution.py:53
  8.7 123.3 %reduce-scatter.4.cloned.1.call-start = ((), (), s32[]{:S(2)}) async-start(), calls=%async_computation.6 | async-start | bytes 2228224 | tf_op jit(solution)/shard_map/reduce_scatter | solution.py:74
  9.0 1.2 copy-start.2
  10.5 0.7 copy-start.15
  11.4 0.9 copy-start.16
  22.9 1.6 copy-start.5
  24.5 2.8 copy-start.8
  31.4 8.9 %copy-start.7 = (bf16[2048,256]{1,0:T(8,128)(2,1)S(1)}, bf16[2048,256]{1,0:T(8,128)(2,1)}, u32[]{:S(2)}) copy-start(bf16[2048,256]{1,0:T(8,128)(2,1)} %param.22) | copy-start | bytes 3145732
  49.1 82.9 %copy-start.11 = (f32[16,1024]{1,0:T(8,128)S(1)}, f32[16,1024]{1,0:T(8,128)}, u32[]{:S(2)}) copy-start(f32[16,1024]{1,0:T(8,128)} %param.29) | copy-start | bytes 196612
  49.1 82.9 %copy-start.12 = (f32[16,1024]{1,0:T(8,128)S(1)}, f32[16,1024]{1,0:T(8,128)}, u32[]{:S(2)}) copy-start(f32[16,1024]{1,0:T(8,128)} %param.27) | copy-start | bytes 196612
  49.1 82.9 %copy-start.13 = (f32[16,1024]{1,0:T(8,128)S(1)}, f32[16,1024]{1,0:T(8,128)}, u32[]{:S(2)}) copy-start(f32[16,1024]{1,0:T(8,128)} %param.28) | copy-start | bytes 196612
  49.1 82.9 %copy-start.14 = (f32[16,1024]{1,0:T(8,128)S(1)}, f32[16,1024]{1,0:T(8,128)}, u32[]{:S(2)}) copy-start(f32[16,1024]{1,0:T(8,128)} %param.26) | copy-start | bytes 196612
  49.2 143.0 %copy-start.9 = (f32[128,1024]{1,0:T(8,128)S(1)}, f32[128,1024]{1,0:T(8,128)}, u32[]{:S(2)}) copy-start(f32[128,1024]{1,0:T(8,128)} %param.24) | copy-start | bytes 1572868
  49.2 145.9 %copy-start.10 = (f32[1024,128]{1,0:T(8,128)S(1)}, f32[1024,128]{1,0:T(8,128)}, u32[]{:S(2)}) copy-start(f32[1024,128]{1,0:T(8,128)} %param.25) | copy-start | bytes 1572868
  49.2 143.0 %all-gather.10.cloned.1.call-start = ((), (), s32[]{:S(2)}) async-start(), calls=%async_computation.3 | async-start | bytes 2228224 | tf_op jit(solution)/shard_map/all_gather | solution.py:80
  133.7 136.1 %all-gather.12.cloned.1.call-start = ((), (), s32[]{:S(2)}) async-start(), calls=%async_computation.4 | async-start | bytes 4456448 | tf_op jit(solution)/shard_map/all_gather | solution.py:96
  192.2 2.9 copy-start.6
  195.0 165.3 %all-gather.14.cloned.1.call-start = ((), (), s32[]{:S(2)}) async-start(), calls=%async_computation.5 | async-start | bytes 4456448 | tf_op jit(solution)/shard_map/all_gather | solution.py:97
  360.3 4.8 %copy-start.4 = (bf16[1024,2048]{1,0:T(8,128)(2,1)S(1)}, bf16[1024,2048]{1,0:T(8,128)(2,1)}, u32[]{:S(2)}) copy-start(bf16[1024,2048]{1,0:T(8,128)(2,1)} %all-gather.14.cloned.1.call-done) | copy-start | bytes 12582916
  365.1 2.0 copy-start.1
Sparse Core Ops, SparseCore 0:
  9.5 13.2 all-gather.7
  24.4 11.7 all-gather.5
  49.3 82.6 reduce-scatter.3
  135.2 56.9 all-gather.9
  195.4 74.3 all-gather.11
  272.9 87.3 all-gather.13
where the time goes:
time: 374 us
  waiting for transfers between devices  319 us (85%)
  matrix products  23.3 us (6%)
  between operations  14.3 us (4%)
  local copies, waits for them, and re-layouts  13.8 us (4%)
    all_gather x1, waiting for transfers between devices, local(): lax.all_gather(output_master.astype(jnp.bfloat16), 'fs', axis=1, tiled=True)  90.5 us
    reduce_scatter x1, waiting for transfers between devices, local(): lax.psum_scatter(partial_value, 'fs', scatter_dimension=0, tiled=True)  82.7 us
    all_gather x1, waiting for transfers between devices, local(): lax.all_gather(value_master.astype(jnp.bfloat16), 'fs', axis=0, tiled=True)  70.7 us
    all_gather x1, waiting for transfers between devices, local(): full_direction = lax.all_gather(direction, 'fs', axis=0, tiled=True)  58.5 us
    unnamed x39, local copies, waits for them, and re-layouts  11.6 us
    dot_general x2, matrix products, contract_rows(): lax.dot_general(left, right, (((0,), (0,)), ((), ())), precision=lax.Prec...  10.9 us
    all_gather x1, waiting for transfers between devices, local(): lax.all_gather(output_cotangent, 'tp', axis=1, tiled=True)  10.5 us
  transfers between devices with their start and end apart: 6, of which 6 were waited for; matrix products, arithmetic and copies ran while one was open for 4% of the time, Pallas kernels for 0%

commit v1 on v0

--- a/solution.py
+++ b/solution.py
@@ -94,7 +94,7 @@
     output_master = output_weight - 0.05 * step_output.T
     value_copy, output_copy = (
         lax.all_gather(value_master.astype(jnp.bfloat16), "fs", axis=0, tiled=True),
-        lax.all_gather(output_master.astype(jnp.bfloat16), "fs", axis=1, tiled=True),
+        jnp.concatenate(lax.all_gather(output_master.astype(jnp.bfloat16), "fs"), axis=1),
     )
     return (
         value_master,

time: 374 us -> 359 us (0.960)
  waiting for transfers between devices: 319 us -> 301 us
    all_gather x1, waiting for transfers between devices: 90.5 us -> 70.9 us  [local(): lax.all_gather(output_master.astype(jnp.bfloat16), 'fs')]
    reshape x0 -> x1, local copies, waits for them, and re-layouts: none -> 5.4 us  [local(): jnp.concatenate(lax.all_gather(output_master.astype(jnp.bfloat16), 'fs'),...]
    unnamed x39 -> x36, local copies, waits for them, and re-layouts: 11.6 us -> 9.46 us
  transfers between devices with their start and end apart: 6 -> 6, of which waited for: 6 -> 6; matrix products, arithmetic and copies ran while one was open for 4% -> 5% of each run, Pallas kernels for 0% -> 0%
where the time goes in v1:
time: 359 us
  waiting for transfers between devices  301 us (84%)
  matrix products  23.3 us (6%)
  local copies, waits for them, and re-layouts  17.1 us (5%)
  between operations  14.3 us (4%)
    reduce_scatter x1, waiting for transfers between devices, local(): lax.psum_scatter(partial_value, 'fs', scatter_dimension=0, tiled=True)  82.7 us
    all_gather x1, waiting for transfers between devices, local(): lax.all_gather(value_master.astype(jnp.bfloat16), 'fs', axis=0, tiled=True)  72 us
    all_gather x1, waiting for transfers between devices, local(): lax.all_gather(output_master.astype(jnp.bfloat16), 'fs')  70.9 us
    all_gather x1, waiting for transfers between devices, local(): full_direction = lax.all_gather(direction, 'fs', axis=0, tiled=True)  58.5 us
    dot_general x2, matrix products, contract_rows(): lax.dot_general(left, right, (((0,), (0,)), ((), ())), precision=lax.Prec...  10.9 us
    all_gather x1, waiting for transfers between devices, local(): lax.all_gather(output_cotangent, 'tp', axis=1, tiled=True)  10.5 us
    unnamed x36, local copies, waits for them, and re-layouts  9.46 us
  transfers between devices with their start and end apart: 6, of which 6 were waited for; matrix products, arithmetic and copies ran while one was open for 5% of the time, Pallas kernels for 0%

profile of v1, /device:TPU:0, one launch (start us, length us, event | category | flops | bytes accessed | tf_op | source)
XLA Modules:
  0.0 359.0 jit_solution(16300867602004789932)
XLA Ops:
  7.2 0.7 all-gather.9.cloned.1.call-update
  8.0 0.7 all-gather.7.cloned.1.call-update
  9.5 0.7 copy-done.2
  11.4 0.6 multiply_reduce_fusion
  12.4 10.5 %all-gather.9.cloned.1.call-done = bf16[512,2048]{1,0:T(8,128)(2,1)} async-done(((bf16[512,1024]{1,0:T(8,128)(2,1)}), bf16[512,2048]{1,0:T(8,128)(2,1)}) %all-gather.9.cloned.1.call-update) | async-done | bytes 2097168 | tf_op jit(solution)/shard_map/all_gather | solution.py:54
  22.9 0.6 mul.105
  23.5 1.0 copy-done.4
  24.5 2.8 fusion.18
  27.3 4.0 %fusion.13 = f32[256,1024]{0,1:T(8,128)S(1)} fusion(bf16[2048,256]{1,0:T(8,128)(2,1)S(1)} %copy-done.6, f32[1024,2048]{1,0:T(8,128)S(1)} %fusion.18), kind=kOutput, calls=%fused_computation.19 | convolution fusion | flops 6444548096 | bytes 10485760 | tf_op jit(solution)/shard_map/dot_general | solution.py:10
  31.4 4.8 %all-gather.7.cloned.1.call-done = bf16[512,2048]{1,0:T(8,128)(2,1)} async-done(((bf16[512,1024]{1,0:T(8,128)(2,1)}), bf16[512,2048]{1,0:T(8,128)(2,1)}) %all-gather.7.cloned.1.call-update) | async-done | bytes 2097168 | tf_op jit(solution)/shard_map/all_gather | solution.py:53
  36.2 4.0 %fusion.38 = f32[2048,1024]{1,0:T(8,128)S(1)} fusion(bf16[512,2048]{1,0:T(8,128)(2,1)} %all-gather.7.cloned.1.call-done, bf16[512,1024]{1,0:T(8,128)(2,1)S(1)} %copy-done), kind=kOutput, calls=%fused_computation.48 | convolution fusion | flops 2147483648 | bytes 11534336 | tf_op jit(solution)/shard_map/dot_general | solution.py:17
  40.2 6.9 %fusion.10 = f32[256,1024]{0,1:T(8,128)S(1)} fusion(bf16[2048,256]{1,0:T(8,128)(2,1)S(1)} %copy-done.7, f32[2048,1024]{1,0:T(8,128)S(1)} %fusion.38), kind=kOutput, calls=%fused_computation.18 | convolution fusion | flops 6444548096 | bytes 10485760 | tf_op jit(solution)/shard_map/dot_general | solution.py:10
  47.3 1.8 copy.53
  49.3 82.7 %reduce-scatter.4.cloned.1.call-done = f32[16,2048]{1,0:T(8,128)} async-done(((f32[256,2048]{1,0:T(8,128)}), f32[16,2048]{1,0:T(8,128)}) %reduce-scatter.4.cloned.1.call-update) | async-done | bytes 131088 | tf_op jit(solution)/shard_map/reduce_scatter | solution.py:74
  132.0 1.6 add_divide_fusion
  133.7 58.5 %all-gather.11.cloned.1.call-done = f32[256,2048]{1,0:T(8,128)} async-done(((f32[16,2048]{1,0:T(8,128)}), f32[256,2048]{1,0:T(8,128)}) %all-gather.11.cloned.1.call-update) | async-done | bytes 2097168 | tf_op jit(solution)/shard_map/all_gather | solution.py:80
  192.2 3.3 fusion.37
  195.6 2.2 fusion.36
  197.8 0.7 fusion.35
  198.5 0.7 fusion.34
  199.1 70.9 %all-gather.15.cloned.1.call-done = bf16[16384,128]{1,0:T(8,128)(2,1)} async-done(((bf16[1024,128]{1,0:T(8,128)(2,1)}), bf16[16384,128]{1,0:T(8,128)(2,1)}) %all-gather.15.cloned.1.call-update) | async-done | bytes 4194320 | tf_op jit(solution)/shard_map/all_gather | solution.py:97
  270.0 5.4 %copy.62 = bf16[16,128,8,128]{3,2,0,1:T(8,128)(2,1)} copy(bf16[16,128,8,128]{3,2,1,0:T(8,128)(2,1)} %bitcast.36) | data formatting | bytes 8388608 | tf_op jit(solution)/shard_map/reshape | solution.py:97
  275.4 72.0 %all-gather.13.cloned.1.call-done = bf16[2048,1024]{1,0:T(8,128)(2,1)} async-done(((bf16[128,1024]{1,0:T(8,128)(2,1)}), bf16[2048,1024]{1,0:T(8,128)(2,1)}) %all-gather.13.cloned.1.call-update) | async-done | bytes 4194320 | tf_op jit(solution)/shard_map/all_gather | solution.py:96
  347.5 4.7 %copy.64 = bf16[2048,1024]{1,0:T(8,128)(2,1)} copy(bf16[2048,1024]{1,0:T(8,128)(2,1)} %all-gather.13.cloned.1.call-done) | data formatting | bytes 8388608
  (50 shorter events, 2.7 us)
Async XLA Ops:
  7.2 29.0 %copy-start = (bf16[512,1024]{1,0:T(8,128)(2,1)S(1)}, bf16[512,1024]{1,0:T(8,128)(2,1)}, u32[]{:S(2)}) copy-start(bf16[512,1024]{1,0:T(8,128)(2,1)} %param.16) | copy-start | bytes 3145732
  7.2 1.5 copy-start.3
  7.2 15.7 %all-gather.9.cloned.1.call-start = ((), (), s32[]{:S(2)}) async-start(), calls=%async_computation.2 | async-start | bytes 3145728 | tf_op jit(solution)/shard_map/all_gather | solution.py:54
  7.9 28.3 %all-gather.7.cloned.1.call-start = ((), (), s32[]{:S(2)}) async-start(), calls=%async_computation.1 | async-start | bytes 3145728 | tf_op jit(solution)/shard_map/all_gather | solution.py:53
  8.7 123.3 %reduce-scatter.4.cloned.1.call-start = ((), (), s32[]{:S(2)}) async-start(), calls=%async_computation.6 | async-start | bytes 2228224 | tf_op jit(solution)/shard_map/reduce_scatter | solution.py:74
  9.0 1.2 copy-start.2
  10.5 0.7 copy-start.14
  11.4 0.9 copy-start.15
  22.9 1.6 copy-start.4
  24.5 2.8 copy-start.6
  31.4 8.9 %copy-start.7 = (bf16[2048,256]{1,0:T(8,128)(2,1)S(1)}, bf16[2048,256]{1,0:T(8,128)(2,1)}, u32[]{:S(2)}) copy-start(bf16[2048,256]{1,0:T(8,128)(2,1)} %param.22) | copy-start | bytes 3145732
  49.1 82.9 %copy-start.10 = (f32[16,1024]{1,0:T(8,128)S(1)}, f32[16,1024]{1,0:T(8,128)}, u32[]{:S(2)}) copy-start(f32[16,1024]{1,0:T(8,128)} %param.29) | copy-start | bytes 196612
  49.1 82.9 %copy-start.11 = (f32[16,1024]{1,0:T(8,128)S(1)}, f32[16,1024]{1,0:T(8,128)}, u32[]{:S(2)}) copy-start(f32[16,1024]{1,0:T(8,128)} %param.27) | copy-start | bytes 196612
  49.1 82.9 %copy-start.12 = (f32[16,1024]{1,0:T(8,128)S(1)}, f32[16,1024]{1,0:T(8,128)}, u32[]{:S(2)}) copy-start(f32[16,1024]{1,0:T(8,128)} %param.28) | copy-start | bytes 196612
  49.1 82.9 %copy-start.13 = (f32[16,1024]{1,0:T(8,128)S(1)}, f32[16,1024]{1,0:T(8,128)}, u32[]{:S(2)}) copy-start(f32[16,1024]{1,0:T(8,128)} %param.26) | copy-start | bytes 196612
  49.2 143.0 %copy-start.8 = (f32[1024,128]{1,0:T(8,128)S(1)}, f32[1024,128]{1,0:T(8,128)}, u32[]{:S(2)}) copy-start(f32[1024,128]{1,0:T(8,128)} %param.25) | copy-start | bytes 1572868
  49.2 146.3 %copy-start.9 = (f32[128,1024]{1,0:T(8,128)S(1)}, f32[128,1024]{1,0:T(8,128)}, u32[]{:S(2)}) copy-start(f32[128,1024]{1,0:T(8,128)} %param.24) | copy-start | bytes 1572868
  49.2 143.0 %all-gather.11.cloned.1.call-start = ((), (), s32[]{:S(2)}) async-start(), calls=%async_computation.3 | async-start | bytes 2228224 | tf_op jit(solution)/shard_map/all_gather | solution.py:80
  133.7 136.4 %all-gather.15.cloned.1.call-start = ((), (), s32[]{:S(2)}) async-start(), calls=%async_computation.5 | async-start | bytes 4456448 | tf_op jit(solution)/shard_map/all_gather | solution.py:97
  192.2 3.4 copy-start.5
  195.5 152.0 %all-gather.13.cloned.1.call-start = ((), (), s32[]{:S(2)}) async-start(), calls=%async_computation.4 | async-start | bytes 4456448 | tf_op jit(solution)/shard_map/all_gather | solution.py:96
  347.5 4.7 %copy-start.1 = (bf16[512,1024]{1,0:T(8,128)(2,1)S(1)}, bf16[512,1024]{1,0:T(8,128)(2,1)}, u32[]{:S(2)}) copy-start(bf16[512,1024]{1,0:T(8,128)(2,1)} %param.16) | copy-start | bytes 3145732
Sparse Core Ops, SparseCore 0:
  9.5 13.2 all-gather.8
  24.4 11.7 all-gather.6
  49.3 82.6 reduce-scatter.3
  135.2 56.9 all-gather.10
  195.6 74.3 all-gather.14
  273.2 74.1 all-gather.12
